TPU v7x, 512 devices: a whole 4x8x8 slice. The times are simulated.
512 devices in a mesh: sp: 64 (over z, y), fs: 4 (over x), tp: 2 (over core).
Axes of the slice: x: 4, y: 8, z: 8, core: 2. Of those that a mesh axis runs over, the one named last changes fastest.
Arguments:
- tokens: bfloat16 [4, 8192, 2048], P('fs', ('sp', 'tp')), may hold values from -6 to 6
- norm_gain: float32 [2048], replicated, may hold values from 0.1 to 1.9
- gla_query_weight: bfloat16 [2048, 512], P('sp', 'tp'), may hold values from -0.125 to 0.125
- gla_key_weight: bfloat16 [2048, 512], P('sp', 'tp'), may hold values from -0.125 to 0.125
- gla_value_weight: bfloat16 [2048, 1024], P('sp', 'tp'), may hold values from -0.125 to 0.125
- decay_down: bfloat16 [2048, 32], P('sp'), may hold values from -0.125 to 0.125
- decay_up: bfloat16 [32, 512], P(None, 'tp'), may hold values from -1 to 1
- decay_bias: float32 [512], P('tp'), may hold values from 0.5 to 12
- head_gain: float32 [128], replicated, may hold values from 0.1 to 1.9
- window_query_weight: bfloat16 [2048, 1024], P('sp', 'tp'), may hold values from -3 to 3
- window_key_weight: bfloat16 [2048, 256], P('sp', 'tp'), may hold values from -3 to 3
- window_value_weight: bfloat16 [2048, 256], P('sp', 'tp'), may hold values from -0.125 to 0.125
- sink_logit: float32 [16], P('tp'), may hold values from 3 to 7
- gla_output_weight: bfloat16 [1024, 2048], P('tp', 'sp'), may hold values from -0.125 to 0.125
- window_output_weight: bfloat16 [1024, 2048], P('tp', 'sp'), may hold values from -0.125 to 0.125
Outputs:
- mixed: bfloat16 [4, 8192, 2048], P('fs', ('sp', 'tp'))
All inputs are finite; a program needn't handle non-finite values.
Results may differ from a plain program's by a relative error of at most 0.013.
Values may be sent and summed in bfloat16 or wider, within the bound.
A program may use at most 64 MiB of HBM per device.

v0:
```python
import jax
import jax.numpy as jnp
from jax import lax
from jax.sharding import Mesh
from jax.sharding import PartitionSpec as P

KEY_DIM = 64
VALUE_DIM = 128
SWA_HEADS = 16
KV_HEADS = 4
HEAD_DIM = 64
WINDOW = 128
SPAN = 64
SP = ("sp_0", "sp_1")
SP_TP = ("sp_0", "sp_1", "tp")
EPS = 1e-06
SOFTMAX_TEMPER = 16.0
HIGH = lax.Precision.HIGHEST


def sent_to_all(value, axis):
    peers = lax.axis_size(axis)
    return lax.all_to_all(
        jnp.broadcast_to(value[None], (peers, *value.shape)), axis, 0, 0, tiled=True
    )


def laid_out(blocks, dim):
    dims = list(blocks.shape[1:])
    dims[dim] *= blocks.shape[0]
    return jnp.moveaxis(blocks, 0, dim).reshape(dims)


def gather_directly(value, axis, dim):
    blocks = sent_to_all(value, axis)
    return laid_out(blocks, dim)


def side_by_side(arrays, axis, dim, along):
    both = jnp.concatenate(arrays, axis=along)
    result, at, finished = (lax.all_gather(both, axis, axis=dim, tiled=True), 0, [])
    for a in arrays:
        finished.append(lax.slice_in_dim(result, at, at + a.shape[along], axis=along))
        at += a.shape[along]
    return tuple(finished)


def gather_turned(arrays, axis, dims):
    turned = [jnp.moveaxis(a, dim, 0) for a, dim in zip(arrays, dims)]
    both = jnp.concatenate([t.reshape(len(t), -1) for t in turned], axis=1)
    result, at, finished = (lax.all_gather(both, axis, axis=0, tiled=True), 0, [])
    for t, dim in zip(turned, dims):
        slab = result[:, at : at + t[0].size].reshape(-1, *t.shape[1:])
        finished.append(jnp.moveaxis(slab, 0, dim))
        at += t[0].size
    return tuple(finished)


def nothing_yet(value, identity):
    return jax.tree.map(
        lambda a, e: jnp.broadcast_to(jnp.asarray(e, a.dtype), a.shape), value, identity
    )


def carried_in(value, axes, combine, identity):
    before = start = nothing_yet(value, identity)
    subtotal = value
    for axis in reversed(axes):
        peers, place = (lax.axis_size(axis), lax.axis_index(axis))
        pieces = jax.tree.map(lambda part: lax.all_gather(part, axis), subtotal)
        inside, subtotal = (start, start)
        for k in range(peers):
            passed = k < place
            subtotal = combine(subtotal, jax.tree.map(lambda part: part[k], pieces))
            inside = jax.tree.map(lambda new, old: jnp.where(passed, new, old), subtotal, inside)
        before = combine(inside, before)
    return before


def passed_along(value, axis, by):
    peers = lax.axis_size(axis)
    pairs = [(i, i + by) for i in range(peers) if 0 <= i + by < peers]
    return lax.ppermute(value, axis, pairs)


def split_up(value, dim, peers):
    dims = value.shape
    blocks = value.reshape(*dims[:dim], peers, dims[dim] // peers, *dims[dim + 1 :])
    return jnp.moveaxis(blocks, dim, 0)


def summed_on_arrival(value, axis, dim):
    blocks = split_up(value, dim, lax.axis_size(axis))
    arrived = lax.all_to_all(blocks, axis, split_axis=0, concat_axis=0, tiled=True)
    return arrived.astype(jnp.float32).sum(axis=0)


def rms_rows(values, gain):
    mean_square = jnp.mean(values * values, axis=-1, keepdims=True)
    return values * lax.rsqrt(mean_square + EPS) * gain


def block_terms(query_rows, key_rows, value_rows, log_decay_rate, block_len):
    seq_len, head_count, key_width = query_rows.shape
    value_width = value_rows.shape[-1]
    block_count = seq_len // block_len
    q_scaled = query_rows.reshape(block_count, block_len, head_count, key_width) * key_width ** (
        -0.5
    )
    k_blocks = key_rows.reshape(block_count, block_len, head_count, key_width)
    v_blocks = value_rows.reshape(block_count, block_len, head_count, value_width)
    within = jnp.cumsum(
        log_decay_rate.reshape(block_count, block_len, head_count, key_width), axis=1
    )
    block_total = within[:, -1]
    q_dec = q_scaled * jnp.exp(within)
    k_dec = k_blocks * jnp.exp(-within)
    k_end = k_blocks * jnp.exp(block_total[:, None] - within)
    causal = jnp.tril(jnp.ones((block_len, block_len), dtype=bool))
    scores = jnp.einsum("nihd,njhd->nhij", q_dec, k_dec, precision=HIGH)
    scores = jnp.where(causal, scores, 0.0)
    local_out = jnp.einsum("nhij,njhe->nihe", scores, v_blocks, precision=HIGH)
    update = jnp.einsum("njhd,njhe->nhde", k_end, v_blocks, precision=HIGH)

    def advance(carried, inputs):
        update_in, decay_in = inputs
        return (decay_in[..., None] * carried + update_in, carried)

    start_state = jnp.zeros((head_count, key_width, value_width), jnp.float32)
    last_state, entering = lax.scan(advance, start_state, (update, jnp.exp(block_total)))
    return (q_dec, local_out, entering, last_state, block_total)


def window_band_mask(block_count, block_len, offset):
    query_pos = jnp.arange(block_len)[:, None] + block_len
    key_pos = jnp.arange(2 * block_len)[None, :]
    distance = query_pos - key_pos
    inside = (distance >= 0) & (distance < block_len)
    global_key = (
        offset + jnp.arange(block_count)[:, None, None] * block_len - block_len + key_pos[None]
    )
    return inside[None] & (global_key >= 0)


def window_attend(query_blocks, key_band, value_band, valid, sinks):
    scores = jnp.einsum(
        "nqhgd,nkhd->nhgqk", query_blocks, key_band, preferred_element_type=jnp.float32
    )
    scores = scores * HEAD_DIM ** (-0.5)
    scores = jnp.where(valid[:, None, None], scores, -1e30)
    sink_term = sinks[None, :, :, None, None]
    top = jnp.maximum(jnp.max(scores, axis=-1, keepdims=True), sink_term)
    expo = jnp.exp(scores - top)
    denom = jnp.sum(expo, axis=-1, keepdims=True) + jnp.exp(sink_term - top)
    weights = (expo / denom).astype(jnp.bfloat16)
    attended = jnp.einsum(
        "nhgqk,nkhd->nqhgd", weights, value_band, preferred_element_type=jnp.float32
    )
    return attended.astype(jnp.bfloat16)


def per_device(
    tokens,
    norm_gain,
    gla_query_weight,
    gla_key_weight,
    gla_value_weight,
    decay_down,
    decay_up,
    decay_bias,
    head_gain,
    window_query_weight,
    window_key_weight,
    window_value_weight,
    sink_logit,
    gla_output_weight,
    window_output_weight,
):
    seq_rows = gather_directly(tokens, "tp", 1)[0]
    tok_rows = seq_rows.shape[0]
    input_maps = side_by_side(
        (
            gla_query_weight,
            gla_key_weight,
            gla_value_weight,
            decay_down,
            window_query_weight,
            window_key_weight,
            window_value_weight,
        ),
        SP,
        0,
        1,
    )
    output_maps = gather_turned((gla_output_weight, window_output_weight), SP, (1, 1))
    normed = rms_rows(seq_rows.astype(jnp.float32), norm_gain).astype(jnp.bfloat16)

    def project(weight):
        return jnp.dot(normed, weight, preferred_element_type=jnp.float32).astype(jnp.bfloat16)

    seq_offset = lax.axis_index(SP) * tok_rows
    window_query = project(input_maps[4])
    sliding_key = project(input_maps[5])
    window_value = project(input_maps[6])
    kv_local = sliding_key.shape[1] // HEAD_DIM
    group_size = SWA_HEADS // KV_HEADS
    block_count = tok_rows // WINDOW
    edge_keys, edge_values = passed_along((sliding_key, window_value), SP, 1)

    def banded(rows, edge_rows):
        blocks = rows.reshape(block_count, WINDOW, kv_local, HEAD_DIM)
        edge_block = edge_rows.reshape(1, WINDOW, kv_local, HEAD_DIM)
        earlier = jnp.concatenate([edge_block, blocks[:-1]], axis=0)
        return jnp.concatenate([earlier, blocks], axis=1)

    query_blocks = window_query.reshape(block_count, WINDOW, kv_local, group_size, HEAD_DIM)
    valid = window_band_mask(block_count, WINDOW, seq_offset)
    sinks = sink_logit.reshape(kv_local, group_size)
    attended = window_attend(
        query_blocks,
        banded(sliding_key, edge_keys),
        banded(window_value, edge_values),
        valid,
        sinks,
    )
    window_hidden = attended.reshape(tok_rows, kv_local * group_size * HEAD_DIM)
    gla_query = project(input_maps[0])
    gla_key = project(input_maps[1])
    gla_value = project(input_maps[2])
    low_rank = project(input_maps[3])
    gate_logit_values = jnp.dot(low_rank, decay_up, preferred_element_type=jnp.float32) + decay_bias
    log_decay_rate = jax.nn.log_sigmoid(gate_logit_values) / SOFTMAX_TEMPER
    local_heads = gla_query.shape[1] // KEY_DIM
    q_dec, local_out, entering, last_state, block_total = block_terms(
        gla_query.astype(jnp.float32).reshape(tok_rows, local_heads, KEY_DIM),
        gla_key.astype(jnp.float32).reshape(tok_rows, local_heads, KEY_DIM),
        gla_value.astype(jnp.float32).reshape(tok_rows, local_heads, VALUE_DIM),
        log_decay_rate.reshape(tok_rows, local_heads, KEY_DIM),
        SPAN,
    )
    device_decay = jnp.exp(jnp.sum(block_total, axis=0))

    def combine(earlier, later):
        return (later[1][..., None] * earlier[0] + later[0], earlier[1] * later[1])

    identity = (jnp.zeros_like(last_state), jnp.ones_like(device_decay))
    incoming = carried_in((last_state, device_decay), SP, combine, identity)[0]
    before = jnp.cumsum(block_total, axis=0) - block_total
    entering_all = entering + jnp.exp(before)[..., None] * incoming[None]
    gla_out = local_out + jnp.einsum("nihd,nhde->nihe", q_dec, entering_all, precision=HIGH)
    gla_out = gla_out.reshape(tok_rows, local_heads, VALUE_DIM)
    gla_hidden = (
        rms_rows(gla_out, head_gain).astype(jnp.bfloat16).reshape(tok_rows, local_heads * VALUE_DIM)
    )
    own_rows = tok_rows // lax.axis_size("tp")
    total = jnp.dot(gla_hidden, output_maps[0], preferred_element_type=jnp.float32)
    mixed = summed_on_arrival(
        (total + jnp.dot(window_hidden, output_maps[1], preferred_element_type=jnp.float32)).astype(
            jnp.bfloat16
        ),
        "tp",
        0,
    )
    return mixed.astype(jnp.bfloat16).reshape(1, own_rows, mixed.shape[1])


def solution(mesh):
    split = Mesh(
        mesh.devices.reshape(8, 8, mesh.shape["fs"], mesh.shape["tp"]), ("sp_0", "sp_1", "fs", "tp")
    )
    return jax.shard_map(
        per_device,
        mesh=split,
        in_specs=(
            P("fs", SP_TP, None),
            P(),
            P(SP, "tp"),
            P(SP, "tp"),
            P(SP, "tp"),
            P(SP, None),
            P(None, "tp"),
            P("tp"),
            P(),
            P(SP, "tp"),
            P(SP, "tp"),
            P(SP, "tp"),
            P("tp"),
            P("tp", SP),
            P("tp", SP),
        ),
        out_specs=P("fs", SP_TP, None),
        check_vma=False,
    )
```

profile of v0, /device:TPU:1, one launch (start us, length us, event | category | flops | bytes accessed | tf_op | source)
XLA Modules:
  0.0 308.5 jit_solution(5424452987641162957)
XLA Ops:
  6.5 1.6 concatenate.12
  8.2 1.8 broadcast_in_dim.36
  10.0 10.3 %all-to-all-start = ((bf16[2,1,64,2048]{3,2,1,0:T(8,128)(2,1)}), bf16[2,1,64,2048]{3,2,1,0:T(8,128)(2,1)S(1)}, u32[]{:S(2)}, u32[]{:S(2)}) async-start(bf16[2,1,64,2048]{3,2,1,0:T(8,128)(2,1)} %broadcast_in_dim.36), calls=%async_computation | async-start | bytes 1048576 | tf_op jit(solution)/shard_map/all_to_all | solution.py:23
  20.3 1.4 all-to-all-done
  22.0 0.9 fusion.25
  22.9 89.3 %all-gather.8.cloned.1.call-done = bf16[2048,1824]{1,0:T(8,128)(2,1)} async-done(((bf16[32,1824]{1,0:T(8,128)(2,1)}), bf16[2048,1824]{1,0:T(8,128)(2,1)}) %all-gather.8.cloned.1.call-update) | async-done | bytes 7471120 | tf_op jit(solution)/shard_map/all_gather | solution.py:41
  112.2 1.6 fusion.43
  114.2 1.5 fusion.20
  115.9 1.5 fusion.18
  117.6 2.0 fusion.11
  119.9 0.4 fusion.34
  120.3 0.4 while.13
  120.7 0.6 copy-done.1
  121.4 18.4 %all-gather.2 = f32[8,4,64]{2,1,0:T(4,128)S(1)} all-gather(f32[1,4,64]{2,1,0:T(4,128)S(1)} %exponential_bitcast_fusion), channel_id=2, replica_groups=mesh['sp_0'=8,'sp_1'=8,'fs'=4,'tp'=2] {'sp_1'}, dimensions={0}, use_global_device_ids=true | all-gather | bytes 9216 | tf_op jit(solution)/shard_map/all_gather | solution.py:70
  139.8 15.8 %all-gather.14.cloned.1.call-done = f32[32,64,128]{2,1,0:T(8,128)} async-done(((f32[4,64,128]{2,1,0:T(8,128)}), f32[32,64,128]{2,1,0:T(8,128)}) %all-gather.14.cloned.1.call-update) | async-done | bytes 1048592 | tf_op jit(solution)/shard_map/all_gather | solution.py:70
  155.7 2.4 fusion.48
  158.1 0.6 pad_maximum_fusion
  159.1 1.9 convolution_convert_fusion.3
  160.9 2.7 collective-permute-start.1
  163.7 19.2 %all_gather.26 = f32[8,4,64]{2,1,0:T(4,128)S(1)} all-gather(f32[1,4,64]{2,1,0:T(4,128)S(1)} %get-tuple-element.80), channel_id=1, replica_groups=mesh['sp_0'=8,'sp_1'=8,'fs'=4,'tp'=2] {'sp_0'}, dimensions={0}, use_global_device_ids=true | all-gather | bytes 9216 | tf_op jit(solution)/shard_map/all_gather | solution.py:70
  182.9 0.5 convolution_select_fusion
  183.7 1.9 convolution_convert_fusion.4
  185.6 2.6 fusion.14
  188.4 2.4 collective-permute-start
  192.1 7.2 %all-gather.10.cloned.1.call-done = f32[8,4,64,128]{3,2,1,0:T(8,128)} async-done(((f32[1,4,64,128]{3,2,1,0:T(8,128)}), f32[8,4,64,128]{3,2,1,0:T(8,128)}) %all-gather.10.cloned.1.call-update) | async-done | bytes 1048592 | tf_op jit(solution)/shard_map/all_gather | solution.py:70
  199.3 1.9 fusion.47
  201.2 0.6 multiply_reduce_fusion.1
  202.1 85.4 %all-gather.12.cloned.1.call-done = bf16[2048,1024]{1,0:T(8,128)(2,1)} async-done(((bf16[32,1024]{1,0:T(8,128)(2,1)}), bf16[2048,1024]{1,0:T(8,128)(2,1)}) %all-gather.12.cloned.1.call-update) | async-done | bytes 4194320 | tf_op jit(solution)/shard_map/all_gather | solution.py:51
  287.7 2.4 fusion.4
  290.1 2.4 fusion
  292.6 8.6 %all_to_all.10 = bf16[2,64,2048]{2,1,0:T(8,128)(2,1)S(1)} all-to-all(bf16[2,64,2048]{2,1,0:T(8,128)(2,1)S(1)} %bitcast.233), channel_id=1, replica_groups=mesh['sp_0'=8,'sp_1'=8,'fs'=4,'tp'=2] {'tp'}, dimensions={0} | all-to-all | bytes 1048576 | tf_op jit(solution)/shard_map/all_to_all | solution.py:94
  301.1 0.8 reduce_sum.52
  (66 shorter events, 4.0 us)
Async XLA Ops:
  6.5 105.7 %copy-start = (bf16[32,256]{1,0:T(8,128)(2,1)S(1)}, bf16[32,256]{1,0:T(8,128)(2,1)}, u32[]{:S(2)}) copy-start(bf16[32,256]{1,0:T(8,128)(2,1)} %param.23) | copy-start | bytes 49156
  6.5 105.7 %all-gather.8.cloned.1.call-start = ((), (), s32[]{:S(2)}) async-start(), calls=%async_computation.2 | async-start | bytes 7987200 | tf_op jit(solution)/shard_map/all_gather | solution.py:41
  10.0 11.7 %all-to-all-start = ((bf16[2,1,64,2048]{3,2,1,0:T(8,128)(2,1)}), bf16[2,1,64,2048]{3,2,1,0:T(8,128)(2,1)S(1)}, u32[]{:S(2)}, u32[]{:S(2)}) async-start(bf16[2,1,64,2048]{3,2,1,0:T(8,128)(2,1)} %broadcast_in_dim.36), calls=%async_computation | async-start | bytes 1048576 | tf_op jit(solution)/shard_map/all_to_all | solution.py:23
  20.3 135.4 %all-gather.14.cloned.1.call-start = ((), (), s32[]{:S(2)}) async-start(), calls=%async_computation.5 | async-start | bytes 1179648 | tf_op jit(solution)/shard_map/all_gather | solution.py:70
  114.1 44.0 %copy-start.4 = (bf16[512,32]{0,1:T(8,128)(2,1)S(1)}, bf16[512,32]{0,1:T(8,128)(2,1)}, u32[]{:S(2)}) copy-start(bf16[512,32]{0,1:T(8,128)(2,1)} %param.31) | copy-start | bytes 98308
  114.1 44.0 %copy-start.5 = (bf16[512,32]{0,1:T(8,128)(2,1)S(1)}, bf16[512,32]{0,1:T(8,128)(2,1)}, u32[]{:S(2)}) copy-start(bf16[512,32]{0,1:T(8,128)(2,1)} %param.30) | copy-start | bytes 98308
  114.1 44.7 %copy-start.7 = (f32[8]{0:T(128)S(1)}, f32[8]{0:T(128)}, u32[]{:S(2)}) copy-start(f32[8]{0:T(128)} %param.29) | copy-start | bytes 100
  114.2 44.8 %copy-start.6 = (f32[128]{0:T(128)S(1)}, f32[128]{0:T(128)}, u32[]{:S(2)}) copy-start(f32[128]{0:T(128)} %param.25) | copy-start | bytes 1540
  120.6 0.7 copy-start.1
  121.3 78.0 %all-gather.10.cloned.1.call-start = ((), (), s32[]{:S(2)}) async-start(), calls=%async_computation.3 | async-start | bytes 1179648 | tf_op jit(solution)/shard_map/all_gather | solution.py:70
  155.7 43.6 %copy-start.2 = (f32[32,64,128]{2,1,0:T(8,128)S(1)}, f32[32,64,128]{2,1,0:T(8,128)}, u32[]{:S(2)}) copy-start(f32[32,64,128]{2,1,0:T(8,128)} %all-gather.14.cloned.1.call-done) | copy-start | bytes 3145732
  158.0 41.3 %copy-start.3 = (f32[1,4,64,128]{3,2,1,0:T(8,128)S(1)}, f32[1,4,64,128]{3,2,1,0:T(8,128)}, u32[]{:S(2)}) copy-start(f32[1,4,64,128]{3,2,1,0:T(8,128)} %get-tuple-element.63) | copy-start | bytes 393220
  158.1 129.4 %all-gather.12.cloned.1.call-start = ((), (), s32[]{:S(2)}) async-start(), calls=%async_computation.4 | async-start | bytes 4259840 | tf_op jit(solution)/shard_map/all_gather | solution.py:51
  160.9 29.8 %collective-permute-start.1 = (bf16[128,128]{0,1:T(8,128)(2,1)S(1)}, bf16[128,128]{0,1:T(8,128)(2,1)S(1)}, u32[]{:S(2)}, u32[]{:S(2)}) collective-permute-start(bf16[128,128]{0,1:T(8,128)(2,1)S(1)} %convolution_convert_fusion.3), channel_id=1, source_target_pairs={{0,8},{8,16},{16,24},{24,32},{32,40},{40,48},{48,56},{56,64},{64,7... | collective-permute-start | bytes 98312 | tf_op jit(solution)/shard_map/ppermute | solution.py:83
  188.4 3.4 %collective-permute-start = (bf16[128,128]{0,1:T(8,128)(2,1)S(1)}, bf16[128,128]{0,1:T(8,128)(2,1)S(1)}, u32[]{:S(2)}, u32[]{:S(2)}) collective-permute-start(bf16[128,128]{0,1:T(8,128)(2,1)S(1)} %convolution_convert_fusion.4), channel_id=1, source_target_pairs={{0,8},{8,16},{16,24},{24,32},{32,40},{40,48},{48,56},{56,64},{64,7... | collective-permute-start | bytes 98312 | tf_op jit(solution)/shard_map/ppermute | solution.py:83
Sparse Core Ops, SparseCore 0:
  10.3 101.8 all-gather.7
  121.4 34.1 all-gather.13
  158.2 41.0 all-gather.9
  202.2 85.2 all-gather.11
where the time goes:
time: 309 us
  waiting for transfers between devices  200 us (65%)
  blocking collectives  46.2 us (15%)
  matrix products  20.4 us (7%)
  starting transfers between devices  15.5 us (5%)
  between operations  13.5 us (4%)
  other arithmetic  7.83 us (3%)
  local copies, waits for them, and re-layouts  5.43 us (2%)
    all_gather x1, waiting for transfers between devices, side_by_side(): lax.all_gather(both, axis, axis=dim, tiled=True)  89.3 us
    all_gather x1, waiting for transfers between devices, gather_turned(): lax.all_gather(both, axis, axis=0, tiled=True)  85.4 us
    all_gather x2, blocking collectives, carried_in(): pieces = jax.tree.map(lambda part: lax.all_gather(part, axis), subtotal)  37.6 us
    all_gather x2, waiting for transfers between devices, carried_in(): pieces = jax.tree.map(lambda part: lax.all_gather(part, axis), subtotal)  23.1 us
    dot_general x6, matrix products, project(): jnp.dot(normed, weight, preferred_element_type=jnp.float32)  11.5 us
    all_to_all x1, starting transfers between devices, sent_to_all(): lax.all_to_all(jnp.broadcast_to(value[None], (peers, *value.shape)), axis...  10.3 us
    all_to_all x1, blocking collectives, summed_on_arrival(): lax.all_to_all(blocks, axis, split_axis=0, concat_axis=0, tiled=True)  8.59 us
  transfers between devices with their start and end apart: 7, of which 6 were waited for; matrix products, arithmetic and copies ran while one was open for 5% of the time, Pallas kernels for 0%

commit v1 on v0

--- a/solution.py
+++ b/solution.py
@@ -18,6 +18,11 @@
 HIGH = lax.Precision.HIGHEST
 
 
+def all_by_exchange(array, mesh_axis, dim):
+    repeated = jnp.stack([array] * lax.axis_size(mesh_axis))
+    return jnp.concatenate(lax.all_to_all(repeated, mesh_axis, 0, 0), axis=dim)
+
+
 def sent_to_all(value, axis):
     peers = lax.axis_size(axis)
     return lax.all_to_all(
@@ -48,7 +53,7 @@
 def gather_turned(arrays, axis, dims):
     turned = [jnp.moveaxis(a, dim, 0) for a, dim in zip(arrays, dims)]
     both = jnp.concatenate([t.reshape(len(t), -1) for t in turned], axis=1)
-    result, at, finished = (lax.all_gather(both, axis, axis=0, tiled=True), 0, [])
+    result, at, finished = (all_by_exchange(both, axis, 0), 0, [])
     for t, dim in zip(turned, dims):
         slab = result[:, at : at + t[0].size].reshape(-1, *t.shape[1:])
         finished.append(jnp.moveaxis(slab, 0, dim))

time: 309 us -> 334 us (1.081)
  waiting for transfers between devices: 200 us -> 212 us
  starting transfers between devices: 15.5 us -> 26.1 us
    all_gather x1, waiting for transfers between devices: 89.3 us -> 175 us  [side_by_side(): lax.all_gather(both, axis, axis=dim, tiled=True)]
    all_gather x1 -> x0, waiting for transfers between devices: 85.4 us -> none  [gather_turned(): lax.all_gather(both, axis, axis=0, tiled=True)]
    all_gather x2, waiting for transfers between devices: 23.1 us -> 36.6 us  [carried_in(): pieces = jax.tree.map(lambda part: lax.all_gather(part, axis), subtotal)]
    all_to_all x0 -> x1, starting transfers between devices: none -> 11.2 us  [all_by_exchange(): return jnp.concatenate(lax.all_to_all(repeated, mesh_axis, 0, 0), axis=dim)]
  transfers between devices with their start and end apart: 7 -> 7, of which waited for: 6 -> 4; matrix products, arithmetic and copies ran while one was open for 5% -> 8% of each run, Pallas kernels for 0% -> 0%
where the time goes in v1:
time: 334 us; the launch traced here: 333 us
  waiting for transfers between devices  212 us (63%)
  blocking collectives  45.4 us (14%)
  starting transfers between devices  26.1 us (8%)
  matrix products  20.4 us (6%)
  between operations  13.5 us (4%)
  local copies, waits for them, and re-layouts  7.92 us (2%)
  other arithmetic  7.29 us (2%)
    all_gather x1, waiting for transfers between devices, side_by_side(): lax.all_gather(both, axis, axis=dim, tiled=True)  175 us
    all_gather x2, waiting for transfers between devices, carried_in(): pieces = jax.tree.map(lambda part: lax.all_gather(part, axis), subtotal)  36.6 us
    all_gather x2, blocking collectives, carried_in(): pieces = jax.tree.map(lambda part: lax.all_gather(part, axis), subtotal)  36.3 us
    dot_general x6, matrix products, project(): jnp.dot(normed, weight, preferred_element_type=jnp.float32)  11.5 us
    all_to_all x1, starting transfers between devices, all_by_exchange(): return jnp.concatenate(lax.all_to_all(repeated, mesh_axis, 0, 0), axis=dim)  11.2 us
    all_to_all x1, starting transfers between devices, sent_to_all(): lax.all_to_all(jnp.broadcast_to(value[None], (peers, *value.shape)), axis...  10.4 us
    all_to_all x1, blocking collectives, summed_on_arrival(): lax.all_to_all(blocks, axis, split_axis=0, concat_axis=0, tiled=True)  9.09 us
  transfers between devices with their start and end apart: 7, of which 4 were waited for; matrix products, arithmetic and copies ran while one was open for 8% of the time, Pallas kernels for 0%

profile of v1, /device:TPU:1, one launch (start us, length us, event | category | flops | bytes accessed | tf_op | source)
XLA Modules:
  0.0 333.0 jit_solution(15246262378807870528)
XLA Ops:
  6.5 1.6 concatenate.12
  8.2 1.9 broadcast_in_dim.36
  10.0 10.4 %all-to-all-start = ((bf16[2,1,64,2048]{3,2,1,0:T(8,128)(2,1)}), bf16[2,1,64,2048]{3,2,1,0:T(8,128)(2,1)S(1)}, u32[]{:S(2)}, u32[]{:S(2)}) async-start(bf16[2,1,64,2048]{3,2,1,0:T(8,128)(2,1)} %broadcast_in_dim.36), calls=%async_computation | async-start | bytes 1048576 | tf_op jit(solution)/shard_map/all_to_all | solution.py:28
  20.5 0.8 pad_maximum_fusion
  21.3 0.6 all-to-all-done
  21.9 2.5 stack.2
  24.3 11.2 %all-to-all-start.1 = ((bf16[64,32,1024]{2,1,0:T(8,128)(2,1)}), bf16[64,32,1024]{2,1,0:T(8,128)(2,1)}, u32[]{:S(2)}, u32[]{:S(2)}) async-start(bf16[64,32,1024]{2,1,0:T(8,128)(2,1)} %stack.2), calls=%async_computation.1 | async-start | bytes 8388608 | tf_op jit(solution)/shard_map/all_to_all | solution.py:23
  36.3 174.8 %all-gather.7.cloned.1.call-done = bf16[2048,1824]{1,0:T(8,128)(2,1)} async-done(((bf16[32,1824]{1,0:T(8,128)(2,1)}), bf16[2048,1824]{1,0:T(8,128)(2,1)}) %all-gather.7.cloned.1.call-update) | async-done | bytes 7471120 | tf_op jit(solution)/shard_map/all_gather | solution.py:46
  211.1 1.6 fusion.43
  212.9 1.5 fusion.20
  214.6 1.5 fusion.18
  216.3 2.0 fusion.11
  218.7 0.4 fusion.34
  219.1 0.4 while.13
  219.5 0.6 copy-done.1
  220.4 1.9 convolution_convert_fusion.3
  222.3 3.0 collective-permute-start.1
  225.3 18.4 %all-gather.2 = f32[8,4,64]{2,1,0:T(4,128)S(1)} all-gather(f32[1,4,64]{2,1,0:T(4,128)S(1)} %exponential_bitcast_fusion), channel_id=2, replica_groups=mesh['sp_0'=8,'sp_1'=8,'fs'=4,'tp'=2] {'sp_1'}, dimensions={0}, use_global_device_ids=true | all-gather | bytes 9216 | tf_op jit(solution)/shard_map/all_gather | solution.py:75
  243.7 17.9 %all_gather.23 = f32[8,4,64]{2,1,0:T(4,128)S(1)} all-gather(f32[1,4,64]{2,1,0:T(4,128)S(1)} %get-tuple-element.80), channel_id=1, replica_groups=mesh['sp_0'=8,'sp_1'=8,'fs'=4,'tp'=2] {'sp_0'}, dimensions={0}, use_global_device_ids=true | all-gather | bytes 9216 | tf_op jit(solution)/shard_map/all_gather | solution.py:75
  261.7 0.5 convolution_select_fusion
  262.5 1.9 convolution_convert_fusion.4
  264.4 2.4 fusion.48
  266.8 2.6 fusion.14
  269.6 1.3 collective-permute-start
  270.9 0.4 fusion.81
  272.2 36.5 %all-gather.9.cloned.1.call-done = f32[8,4,64,128]{3,2,1,0:T(8,128)} async-done(((f32[1,4,64,128]{3,2,1,0:T(8,128)}), f32[8,4,64,128]{3,2,1,0:T(8,128)}) %all-gather.9.cloned.1.call-update) | async-done | bytes 1048592 | tf_op jit(solution)/shard_map/all_gather | solution.py:75
  308.7 1.9 fusion.47
  310.6 0.6 multiply_reduce_fusion.1
  311.7 2.4 fusion.4
  314.1 2.4 fusion
  316.5 9.1 %all_to_all.15 = bf16[2,64,2048]{2,1,0:T(8,128)(2,1)S(1)} all-to-all(bf16[2,64,2048]{2,1,0:T(8,128)(2,1)S(1)} %bitcast.234), channel_id=1, replica_groups=mesh['sp_0'=8,'sp_1'=8,'fs'=4,'tp'=2] {'tp'}, dimensions={0} | all-to-all | bytes 1048576 | tf_op jit(solution)/shard_map/all_to_all | solution.py:99
  325.6 0.8 reduce_sum.52
  (66 shorter events, 3.8 us)
Async XLA Ops:
  6.5 204.6 %copy-start = (bf16[32,256]{1,0:T(8,128)(2,1)S(1)}, bf16[32,256]{1,0:T(8,128)(2,1)}, u32[]{:S(2)}) copy-start(bf16[32,256]{1,0:T(8,128)(2,1)} %param.23) | copy-start | bytes 49156
  6.5 29.4 %copy-start.4 = (f32[2048]{0:T(1024)S(1)}, f32[2048]{0:T(1024)}, u32[]{:S(2)}) copy-start(f32[2048]{0:T(1024)} %param.18) | copy-start | bytes 24580
  6.5 204.5 %all-gather.7.cloned.1.call-start = ((), (), s32[]{:S(2)}) async-start(), calls=%async_computation.3 | async-start | bytes 7987200 | tf_op jit(solution)/shard_map/all_gather | solution.py:46
  10.0 201.1 %copy-start.5 = (f32[256]{0:T(256)S(1)}, f32[256]{0:T(256)}, u32[]{:S(2)}) copy-start(f32[256]{0:T(256)} %param.24) | copy-start | bytes 3076
  10.0 11.8 %all-to-all-start = ((bf16[2,1,64,2048]{3,2,1,0:T(8,128)(2,1)}), bf16[2,1,64,2048]{3,2,1,0:T(8,128)(2,1)S(1)}, u32[]{:S(2)}, u32[]{:S(2)}) async-start(bf16[2,1,64,2048]{3,2,1,0:T(8,128)(2,1)} %broadcast_in_dim.36), calls=%async_computation | async-start | bytes 1048576 | tf_op jit(solution)/shard_map/all_to_all | solution.py:28
  24.3 287.2 %all-to-all-start.1 = ((bf16[64,32,1024]{2,1,0:T(8,128)(2,1)}), bf16[64,32,1024]{2,1,0:T(8,128)(2,1)}, u32[]{:S(2)}, u32[]{:S(2)}) async-start(bf16[64,32,1024]{2,1,0:T(8,128)(2,1)} %stack.2), calls=%async_computation.1 | async-start | bytes 8388608 | tf_op jit(solution)/shard_map/all_to_all | solution.py:23
  35.6 228.8 %all-gather.11.cloned.1.call-start = ((), (), s32[]{:S(2)}) async-start(), calls=%async_computation.5 | async-start | bytes 1179648 | tf_op jit(solution)/shard_map/all_gather | solution.py:75
  36.2 184.0 %copy-start.6 = (f32[128]{0:T(128)S(1)}, f32[128]{0:T(128)}, u32[]{:S(2)}) copy-start(f32[128]{0:T(128)} %param.25) | copy-start | bytes 1540
  36.2 184.0 %copy-start.7 = (f32[8]{0:T(128)S(1)}, f32[8]{0:T(128)}, u32[]{:S(2)}) copy-start(f32[8]{0:T(128)} %param.29) | copy-start | bytes 100
  219.5 0.7 copy-start.1
  220.2 88.6 %all-gather.9.cloned.1.call-start = ((), (), s32[]{:S(2)}) async-start(), calls=%async_computation.4 | async-start | bytes 1179648 | tf_op jit(solution)/shard_map/all_gather | solution.py:75
  222.3 48.6 %collective-permute-start.1 = (bf16[128,128]{0,1:T(8,128)(2,1)S(1)}, bf16[128,128]{0,1:T(8,128)(2,1)S(1)}, u32[]{:S(2)}, u32[]{:S(2)}) collective-permute-start(bf16[128,128]{0,1:T(8,128)(2,1)S(1)} %convolution_convert_fusion.3), channel_id=1, source_target_pairs={{0,8},{8,16},{16,24},{24,32},{32,40},{40,48},{48,56},{56,64},{64,7... | collective-permute-start | bytes 98312 | tf_op jit(solution)/shard_map/ppermute | solution.py:88
  264.4 44.3 %copy-start.2 = (f32[32,64,128]{2,1,0:T(8,128)S(1)}, f32[32,64,128]{2,1,0:T(8,128)}, u32[]{:S(2)}) copy-start(f32[32,64,128]{2,1,0:T(8,128)} %all-gather.11.cloned.1.call-done) | copy-start | bytes 3145732
  266.8 41.9 %copy-start.3 = (f32[1,4,64,128]{3,2,1,0:T(8,128)S(1)}, f32[1,4,64,128]{3,2,1,0:T(8,128)}, u32[]{:S(2)}) copy-start(f32[1,4,64,128]{3,2,1,0:T(8,128)} %get-tuple-element.63) | copy-start | bytes 393220
  269.6 2.3 collective-permute-start
Sparse Core Ops, SparseCore 0:
  10.3 200.6 all-gather.6
  220.3 34.1 all-gather.10
  266.9 41.7 all-gather.8
